TPU v7x, 128 devices: a whole 4x4x4 slice. The times are simulated.
128 devices in a mesh: fs: 16 (over z, y), tp: 8 (over x, core).
Axes of the slice: x: 4, y: 4, z: 4, core: 2. Of those that a mesh axis runs over, the one named last changes fastest.
Arguments:
- tokens: bfloat16 [12288, 2048], P('fs', 'tp'), may hold values from -40 to 40
- gain_one: float32 [2048], P('tp'), may hold values from 0.1 to 1.9
- w_gate: float32 [2048, 3072], P('fs', 'tp'), may hold values from -0.125 to 0.125
- w_up: float32 [2048, 3072], P('fs', 'tp'), may hold values from -0.125 to 0.125
- w_down: float32 [3072, 2048], P('tp', 'fs'), may hold values from -0.109375 to 0.109375
- scale_gate: float32 [3072], P('tp'), may hold values from 0.5 to 2
- scale_up: float32 [3072], P('tp'), may hold values from 0.5 to 2
- scale_down: float32 [2048], P('tp'), may hold values from 0.5 to 2
- gain_mix: float32 [2048], P('tp'), may hold values from 0.1 to 1.9
- w_query: float32 [2048, 2048], P('fs', 'tp'), may hold values from -0.125 to 0.125
- w_key: float32 [2048, 2048], P('fs', 'tp'), may hold values from -0.125 to 0.125
- w_value: float32 [2048, 2048], P('fs', 'tp'), may hold values from -0.125 to 0.125
- w_outgate: float32 [2048, 2048], P('fs', 'tp'), may hold values from -0.125 to 0.125
- scale_query: float32 [2048], P('tp'), may hold values from 0.5 to 2
- scale_key: float32 [2048], P('tp'), may hold values from 0.5 to 2
- scale_value: float32 [2048], P('tp'), may hold values from 0.5 to 2
- scale_outgate: float32 [2048], P('tp'), may hold values from 0.5 to 2
- ret_gain: float32 [2048], P('tp'), may hold values from 0.1 to 1.9
- decay_rate: float32 [8], P('tp'), may hold values from 0 to 2
- w_mix: float32 [2048, 2048], P('tp', 'fs'), may hold values from -0.125 to 0.125
- scale_mix: float32 [2048], P('tp'), may hold values from 0.5 to 2
- gain_two: float32 [2048], P('tp'), may hold values from 0.1 to 1.9
Outputs:
- layer_out: bfloat16 [12288, 2048], P('fs', 'tp')
All inputs are finite; a program needn't handle non-finite values.
Results may differ from a plain program's by a relative error of at most 0.022.
Values may be sent and summed in bfloat16 or wider, within the bound.
A program may use at most 128 MiB of HBM per device.

v0:
```python
import jax
import jax.numpy as jnp
from jax import lax
from jax.sharding import PartitionSpec as P

D = 2048
LEN = 256
BLK = 128
EPS = 1e-06
HEAD_EPS = 0.1


def from_everyone(shard, axis):
    copies = jnp.broadcast_to(shard, (lax.axis_size(axis), *shard.shape))
    return lax.all_to_all(copies, axis, split_axis=0, concat_axis=0, tiled=True)


def taken_together(shard, axis):
    return from_everyone(shard, axis).sum(axis=0)


def in_blocks(shard, dim, length):
    shape = shard.shape
    blocks = shard.reshape(*shape[:dim], length, shape[dim] // length, *shape[dim + 1 :])
    return jnp.moveaxis(blocks, dim, 0)


def sent_and_summed(shard, axis, dim):
    length = lax.axis_size(axis)
    blocks = lax.all_to_all(in_blocks(shard, dim, length), axis, 0, 0, tiled=True)
    return jnp.sum(blocks.astype(jnp.float32), axis=0)


def side_by_side(arrays, axis, dim, along):
    widths = [a.shape[along] for a in arrays]
    both = jnp.concatenate(arrays, axis=along)
    out = lax.all_gather(both, axis, axis=dim, tiled=True)
    return tuple(jnp.split(out, [sum(widths[:k]) for k in range(1, len(widths))], axis=along))


def laid_out(blocks, dim):
    blocks = jnp.moveaxis(blocks, 0, dim)
    shape = blocks.shape
    return blocks.reshape(*shape[:dim], shape[dim] * shape[dim + 1], *shape[dim + 2 :])


def gathered_copies(shard, axis, dim):
    return laid_out(from_everyone(shard, axis), dim)


def rotate_pairs(values):
    paired = values.reshape(values.shape[:-1] + (values.shape[-1] // 2, 2))
    return jnp.stack((-paired[..., 1], paired[..., 0]), axis=-1).reshape(values.shape)


def retain(query_rows, key_rows, value_rows, decay_rate, length, block):
    total_rows = query_rows.shape[0]
    heads = decay_rate.shape[0]
    head_size = query_rows.shape[1] // heads
    sequences = total_rows // length
    nblocks = length // block

    def split_heads(values):
        return values.astype(jnp.float32).reshape(sequences, length, heads, head_size)

    freq = 1.0 / 10000.0 ** jnp.linspace(0.0, 1.0, head_size // 2, dtype=jnp.float32)
    freq = jnp.repeat(freq, 2)
    angles = jnp.arange(length, dtype=jnp.float32)[:, None] * freq[None, :]
    sines = jnp.sin(angles)[None, :, None, :]
    cosines = jnp.cos(angles)[None, :, None, :]
    queries = split_heads(query_rows)
    queries = queries * cosines + rotate_pairs(queries) * sines
    keys_all = split_heads(key_rows) * head_size ** (-0.5)
    keys_all = keys_all * cosines + rotate_pairs(keys_all) * sines
    values_all = split_heads(value_rows)
    log_decay = -decay_rate
    offsets = jnp.arange(block, dtype=jnp.float32)
    distance = offsets[:, None] - offsets[None, :]
    inside = jnp.where(
        distance >= 0, jnp.exp(log_decay[:, None, None] * jnp.maximum(distance, 0.0)), 0.0
    )
    query_decay = jnp.exp(log_decay[None, :] * (offsets[:, None] + 1.0))
    key_decay = jnp.exp(log_decay[None, :] * (block - 1.0 - offsets[:, None]))
    block_decay = jnp.exp(log_decay * block)

    def to_blocks(values):
        return jnp.moveaxis(values.reshape(sequences, nblocks, block, heads, head_size), 1, 0)

    def advance(carried, pieces):
        query_blk, key_blk, value_blk = pieces
        scores = jnp.einsum("snhd,smhd->shnm", query_blk, key_blk) * inside
        within = jnp.einsum("shnm,smhe->snhe", scores, value_blk)
        across = jnp.einsum("snhd,shde->snhe", query_blk, carried) * query_decay[None, :, :, None]
        weighted = key_blk * key_decay[None, :, :, None]
        carried = carried * block_decay[None, :, None, None] + jnp.einsum(
            "smhd,smhe->shde", weighted, value_blk
        )
        return (carried, within + across)

    initial = jnp.zeros((sequences, heads, head_size, head_size), jnp.float32)
    _, results = lax.scan(
        advance, initial, (to_blocks(queries), to_blocks(keys_all), to_blocks(values_all))
    )
    results = jnp.moveaxis(results, 0, 1).reshape(sequences, length, heads, head_size)
    results = results * lax.rsqrt(jnp.mean(results * results, axis=-1, keepdims=True) + HEAD_EPS)
    return results.reshape(total_rows, heads * head_size)


def normed_rows(hidden_in, norm_gain):
    widened = hidden_in.astype(jnp.float32)
    totals = taken_together(jnp.sum(widened * widened, axis=1), "tp")
    scaled = widened * lax.rsqrt(totals / D + EPS)[:, None] * norm_gain
    return lax.all_gather(scaled.astype(jnp.bfloat16), "tp", axis=1, tiled=True)


def summed_share(partial_value):
    rounded = lax.optimization_barrier(partial_value.astype(jnp.bfloat16))
    return sent_and_summed(rounded.astype(jnp.float32).astype(jnp.bfloat16), "tp", 1)


def ffn_gathered(features, gate_low, up_low, down_low, scale_gate, scale_up):
    pieces = side_by_side((gate_low, up_low), "fs", 0, 1)
    gate_add = jnp.dot(features, pieces[0], preferred_element_type=jnp.float32)
    up_add = jnp.dot(features, pieces[1], preferred_element_type=jnp.float32)
    hidden = (jax.nn.silu(gate_add * scale_gate) * (up_add * scale_up)).astype(jnp.bfloat16)
    return jnp.dot(hidden, gathered_copies(down_low, "fs", 1), preferred_element_type=jnp.float32)


def per_device(
    tokens,
    gain_one,
    w_gate,
    w_up,
    w_down,
    scale_gate,
    scale_up,
    scale_down,
    gain_mix,
    w_query,
    w_key,
    w_value,
    w_outgate,
    scale_query,
    scale_key,
    scale_value,
    scale_outgate,
    ret_gain,
    decay_rate,
    w_mix,
    scale_mix,
    gain_two,
):
    norm_one, norm_mix, norm_two, down_cols, mix_cols = (
        gain_one,
        gain_mix,
        gain_two,
        scale_down,
        scale_mix,
    )
    gate_low = w_gate.astype(jnp.bfloat16)
    up_low = w_up.astype(jnp.bfloat16)
    down_low = w_down.astype(jnp.bfloat16)
    ffn_one = ffn_gathered(
        normed_rows(tokens, norm_one), gate_low, up_low, down_low, scale_gate, scale_up
    )
    first = (tokens.astype(jnp.float32) + 0.5 * summed_share(ffn_one) * down_cols).astype(
        jnp.bfloat16
    )
    features = normed_rows(first, norm_mix)
    pieces = side_by_side(
        (
            w_query.astype(jnp.bfloat16),
            w_key.astype(jnp.bfloat16),
            w_value.astype(jnp.bfloat16),
            w_outgate.astype(jnp.bfloat16),
        ),
        "fs",
        0,
        1,
    )
    query_pre, key_pre, value_pre, outgate_pre = tuple(
        (jnp.dot(features, piece, preferred_element_type=jnp.float32) for piece in pieces)
    )
    query_rows = (query_pre * scale_query).astype(jnp.bfloat16)
    key_rows = (key_pre * scale_key).astype(jnp.bfloat16)
    value_rows = (value_pre * scale_value).astype(jnp.bfloat16)
    outgate_rows = (outgate_pre * scale_outgate).astype(jnp.bfloat16)
    retained = retain(query_rows, key_rows, value_rows, decay_rate, LEN, BLK)
    mixed = (retained * ret_gain * jax.nn.silu(outgate_rows.astype(jnp.float32))).astype(
        jnp.bfloat16
    )
    mix_partial = jnp.dot(
        mixed,
        gathered_copies(w_mix.astype(jnp.bfloat16), "fs", 1),
        preferred_element_type=jnp.float32,
    )
    second = (first.astype(jnp.float32) + summed_share(mix_partial) * mix_cols).astype(jnp.bfloat16)
    ffn_two = ffn_gathered(
        normed_rows(second, norm_two), gate_low, up_low, down_low, scale_gate, scale_up
    )
    result = (second.astype(jnp.float32) + 0.5 * summed_share(ffn_two) * down_cols).astype(
        jnp.bfloat16
    )
    return result


def solution(mesh):
    return jax.shard_map(
        per_device,
        mesh=mesh,
        in_specs=(
            P("fs", "tp"),
            P("tp"),
            P("fs", "tp"),
            P("fs", "tp"),
            P("tp", "fs"),
            P("tp"),
            P("tp"),
            P("tp"),
            P("tp"),
            P("fs", "tp"),
            P("fs", "tp"),
            P("fs", "tp"),
            P("fs", "tp"),
            P("tp"),
            P("tp"),
            P("tp"),
            P("tp"),
            P("tp"),
            P("tp"),
            P("tp", "fs"),
            P("tp"),
            P("tp"),
        ),
        out_specs=P("fs", "tp"),
        check_vma=False,
    )
```

profile of v0, /device:TPU:1, one launch (start us, length us, event | category | flops | bytes accessed | tf_op | source)
XLA Modules:
  0.0 379.9 jit_solution(7782225091500418627)
XLA Ops:
  7.9 10.3 %all_to_all.44 = f32[8,1,768]{2,1,0:T(1,128)S(1)} all-to-all(f32[8,1,768]{2,1,0:T(1,128)S(1)} %broadcast_in_dim.23), channel_id=1, replica_groups=mesh['fs'=16,'tp'=8] {'tp'}, dimensions={0} | all-to-all | bytes 49152 | tf_op jit(solution)/shard_map/all_to_all | solution.py:15
  26.1 7.8 %all-to-all-start.1 = ((bf16[16,384,128]{1,2,0:T(8,128)(2,1)}), bf16[16,384,128]{1,2,0:T(8,128)(2,1)S(1)}, u32[]{:S(2)}, u32[]{:S(2)}) async-start(bf16[16,384,128]{1,2,0:T(8,128)(2,1)} %broadcast_in_dim.24), calls=%async_computation.1 | async-start | bytes 3145728 | tf_op jit(solution)/shard_map/all_to_all | solution.py:15
  33.9 18.4 %all-gather.6.cloned.1.call-done = bf16[768,2048]{1,0:T(8,128)(2,1)} async-done(((bf16[768,256]{1,0:T(8,128)(2,1)}), bf16[768,2048]{1,0:T(8,128)(2,1)}) %all-gather.6.cloned.1.call-update) | async-done | bytes 3145744 | tf_op jit(solution)/shard_map/all_gather | solution.py:113
  52.3 50.1 %all-gather.8.cloned.1.call-done = bf16[2048,768]{1,0:T(8,128)(2,1)} async-done(((bf16[128,768]{1,0:T(8,128)(2,1)}), bf16[2048,768]{1,0:T(8,128)(2,1)}) %all-gather.8.cloned.1.call-update) | async-done | bytes 3145744 | tf_op jit(solution)/shard_map/all_gather | solution.py:37
  102.4 5.2 %convolution_multiply_fusion.4 = f32[768,384]{1,0:T(8,128)} fusion(bf16[768,2048]{1,0:T(8,128)(2,1)} %all-gather.6.cloned.1.call-done, bf16[2048,768]{1,0:T(8,128)(2,1)} %all-gather.8.cloned.1.call-done, f32[384]{0:T(512)S(1)} %copy-done.21), kind=kOutput, calls=%fused_computation.47 | convolution fusion | flops 1208254464 | bytes 5899776 | tf_op jit(solution)/shard_map/dot_general | solution.py:123
  108.8 6.7 %convolution_convert_fusion.2 = bf16[768,2048]{1,0:T(8,128)(2,1)S(1)} fusion(bf16[384,2048]{0,1:T(8,128)(2,1)} %bitcast.163, bf16[768,2048]{1,0:T(8,128)(2,1)} %all-gather.6.cloned.1.call-done, bf16[2048,768]{1,0:T(8,128)(2,1)} %all-gather.8.cloned.1.call-done, f32[768,384]{1,0:T(8,128)} %convolution_multiply_fusion.4, f32[384]{0:T(512)S(1)} %copy-done.22), kind=kOutput, calls=%fused_computation.38 | convolution fusion | flops 2419556352 | bytes 10618368 | tf_op jit(solution)/shard_map/dot_general | solution.py:126
  117.4 5.7 %all-to-all-start.2 = ((bf16[8,768,256]{2,1,0:T(8,128)(2,1)}), bf16[8,768,256]{2,1,0:T(8,128)(2,1)S(1)}, u32[]{:S(2)}, u32[]{:S(2)}) async-start(bf16[8,768,256]{2,1,0:T(8,128)(2,1)} %bitcast.116), calls=%async_computation.2 | async-start | bytes 6291456 | tf_op jit(solution)/shard_map/all_to_all | solution.py:30
  123.1 37.4 %all-to-all-done.2 = bf16[8,768,256]{2,1,0:T(8,128)(2,1)S(1)} async-done(((bf16[8,768,256]{2,1,0:T(8,128)(2,1)}), bf16[8,768,256]{2,1,0:T(8,128)(2,1)S(1)}, u32[]{:S(2)}, u32[]{:S(2)}) %all-to-all-start.2) | async-done | bytes 3145760 | tf_op jit(solution)/shard_map/all_to_all | solution.py:30
  161.2 8.0 %all_to_all.45 = f32[8,1,768]{2,1,0:T(1,128)S(1)} all-to-all(f32[8,1,768]{2,1,0:T(1,128)S(1)} %broadcast_in_dim.27), channel_id=1, replica_groups=mesh['fs'=16,'tp'=8] {'tp'}, dimensions={0} | all-to-all | bytes 49152 | tf_op jit(solution)/shard_map/all_to_all | solution.py:15
  172.3 4.3 %all-to-all-start.4 = ((bf16[16,256,128]{1,2,0:T(8,128)(2,1)}), bf16[16,256,128]{1,2,0:T(8,128)(2,1)}, u32[]{:S(2)}, u32[]{:S(2)}) async-start(bf16[16,256,128]{1,2,0:T(8,128)(2,1)} %broadcast_in_dim.31), calls=%async_computation.4 | async-start | bytes 2097152 | tf_op jit(solution)/shard_map/all_to_all | solution.py:15
  178.0 8.5 %multiply_cosine_fusion = (f32[2,128,256]{1,0,2:T(2,128)}, f32[2,128,256]{1,0,2:T(2,128)}, f32[2,128,256]{1,0,2:T(2,128)}) fusion(f32[2,128]{1,0:T(2,128)S(1)} %multiply_add_fusion, f32[256]{0:T(256)S(1)} %mul.470), kind=kLoop, calls=%fused_computation.107 | loop fusion | flops 327680 | bytes 788480 | tf_op jit(solution)/shard_map/cos | solution.py:70
  186.5 12.2 %all-gather.10.cloned.1.call-done = bf16[768,2048]{1,0:T(8,128)(2,1)} async-done(((bf16[768,256]{1,0:T(8,128)(2,1)}), bf16[768,2048]{1,0:T(8,128)(2,1)}) %all-gather.10.cloned.1.call-update) | async-done | bytes 3145744 | tf_op jit(solution)/shard_map/all_gather | solution.py:113
  198.7 4.1 %broadcast_multiply_fusion = (f32[768,256]{1,0:T(8,128)S(1)}, f32[768,256]{1,0:T(8,128)}) fusion(f32[256]{0:T(256)S(1)} %copy-done.24, bf16[768,2048]{1,0:T(8,128)(2,1)} %all-gather.10.cloned.1.call-done, bf16[2048,1024]{1,0:T(8,128)(2,1)} %all-gather.12.cloned.1.call-done), kind=kOutput, calls=%fused_computation.106 | convolution fusion | flops 806092800 | bytes 5768192 | tf_op jit(solution)/shard_map/dot_general | solution.py:182
  205.7 2.2 fusion.41
  213.3 3.3 fusion.39
  218.5 8.8 %while.15 = (s32[]{:T(128)}, f32[3,1,256,256]{3,2,0,1:T(8,128)S(1)}, f32[2,3,128,1,256]{2,4,1,3,0:T(8,128)}, f32[1]{0:T(128)}, f32[2,3,128,1,256]{2,0,3,4,1:T(2,...) while((s32[]{:T(128)}, ...), condition=%wide.region_6.7_spmd.clone.clone.clone, body=%wide.region_5.6_spmd.clone.clone.clone.sunk | while | flops 152257024 | bytes 7998088 | solution.py:101
  230.0 3.2 fusion.66
  233.3 2.2 convolution_convert_fusion.1
  235.7 41.4 %all_to_all.46 = bf16[8,768,256]{2,1,0:T(8,128)(2,1)S(1)} all-to-all(bf16[8,768,256]{2,1,0:T(8,128)(2,1)S(1)} %bitcast.155), channel_id=1, replica_groups=mesh['fs'=16,'tp'=8] {'tp'}, dimensions={0} | all-to-all | bytes 6291456 | tf_op jit(solution)/shard_map/all_to_all | solution.py:30
  278.4 8.1 %all_to_all.47 = f32[8,1,768]{2,1,0:T(1,128)S(1)} all-to-all(f32[8,1,768]{2,1,0:T(1,128)S(1)} %broadcast_in_dim.32), channel_id=1, replica_groups=mesh['fs'=16,'tp'=8] {'tp'}, dimensions={0} | all-to-all | bytes 49152 | tf_op jit(solution)/shard_map/all_to_all | solution.py:15
  287.5 31.1 %all-gather.14.cloned.1.call-done = bf16[768,2048]{1,0:T(8,128)(2,1)} async-done(((bf16[768,256]{1,0:T(8,128)(2,1)}), bf16[768,2048]{1,0:T(8,128)(2,1)}) %all-gather.14.cloned.1.call-update) | async-done | bytes 3145744 | tf_op jit(solution)/shard_map/all_gather | solution.py:113
  318.6 5.3 %convolution_multiply_fusion.2 = f32[768,384]{1,0:T(8,128)} fusion(bf16[768,2048]{1,0:T(8,128)(2,1)} %all-gather.14.cloned.1.call-done, bf16[2048,768]{1,0:T(8,128)(2,1)} %all-gather.8.cloned.1.call-done, f32[384]{0:T(512)S(1)} %copy-done.21), kind=kOutput, calls=%fused_computation.44 | convolution fusion | flops 1208254464 | bytes 5899776 | tf_op jit(solution)/shard_map/dot_general | solution.py:123
  323.8 6.6 %convolution_convert_fusion = bf16[768,2048]{1,0:T(8,128)(2,1)S(1)} fusion(bf16[384,2048]{0,1:T(8,128)(2,1)} %bitcast.164, bf16[768,2048]{1,0:T(8,128)(2,1)} %all-gather.14.cloned.1.call-done, bf16[2048,768]{1,0:T(8,128)(2,1)} %all-gather.8.cloned.1.call-done, f32[768,384]{1,0:T(8,128)} %convolution_multiply_fusion.2, f32[384]{0:T(512)S(1)} %copy-done.23), kind=kOutput, calls=%fused_computation.36 | convolution fusion | flops 2419556352 | bytes 10618368 | tf_op jit(solution)/shard_map/dot_general | solution.py:126
  330.7 41.4 %all_to_all.48 = bf16[8,768,256]{2,1,0:T(8,128)(2,1)S(1)} all-to-all(bf16[8,768,256]{2,1,0:T(8,128)(2,1)S(1)} %bitcast.156), channel_id=1, replica_groups=mesh['fs'=16,'tp'=8] {'tp'}, dimensions={0} | all-to-all | bytes 6291456 | tf_op jit(solution)/shard_map/all_to_all | solution.py:30
  (148 shorter events, 41.6 us)
Async XLA Ops:
  6.5 17.2 %copy-start.13 = (f32[128,256]{1,0:T(8,128)S(1)}, f32[128,256]{1,0:T(8,128)}, u32[]{:S(2)}) copy-start(f32[128,256]{1,0:T(8,128)} %param.34) | copy-start | bytes 393220
  6.5 17.2 %copy-start.14 = (f32[128,256]{1,0:T(8,128)S(1)}, f32[128,256]{1,0:T(8,128)}, u32[]{:S(2)}) copy-start(f32[128,256]{1,0:T(8,128)} %param.35) | copy-start | bytes 393220
  6.5 17.3 %copy-start.15 = (f32[128,256]{1,0:T(8,128)S(1)}, f32[128,256]{1,0:T(8,128)}, u32[]{:S(2)}) copy-start(f32[128,256]{1,0:T(8,128)} %param.36) | copy-start | bytes 393220
  6.5 18.1 %copy-start.12 = (f32[384,128]{1,0:T(8,128)S(1)}, f32[384,128]{1,0:T(8,128)}, u32[]{:S(2)}) copy-start(f32[384,128]{1,0:T(8,128)} %param.28) | copy-start | bytes 589828
  6.5 45.8 %all-gather.6.cloned.1.call-start = ((), (), s32[]{:S(2)}) async-start(), calls=%async_computation.8 | async-start | bytes 3538944 | tf_op jit(solution)/shard_map/all_gather | solution.py:113
  20.1 82.3 %all-gather.8.cloned.1.call-start = ((), (), s32[]{:S(2)}) async-start(), calls=%async_computation.9 | async-start | bytes 3342336 | tf_op jit(solution)/shard_map/all_gather | solution.py:37
  22.8 163.7 %all-gather.12.cloned.1.call-start = ((), (), s32[]{:S(2)}) async-start(), calls=%async_computation.11 | async-start | bytes 4456448 | tf_op jit(solution)/shard_map/all_gather | solution.py:37
  23.8 78.6 %copy-start.21 = (f32[384]{0:T(512)S(1)}, f32[384]{0:T(512)}, u32[]{:S(2)}) copy-start(f32[384]{0:T(512)} %param.29) | copy-start | bytes 4612
  26.1 81.5 %all-to-all-start.1 = ((bf16[16,384,128]{1,2,0:T(8,128)(2,1)}), bf16[16,384,128]{1,2,0:T(8,128)(2,1)S(1)}, u32[]{:S(2)}, u32[]{:S(2)}) async-start(bf16[16,384,128]{1,2,0:T(8,128)(2,1)} %broadcast_in_dim.24), calls=%async_computation.1 | async-start | bytes 3145728 | tf_op jit(solution)/shard_map/all_to_all | solution.py:15
  33.9 74.9 %copy-start.22 = (f32[384]{0:T(512)S(1)}, f32[384]{0:T(512)}, u32[]{:S(2)}) copy-start(f32[384]{0:T(512)} %param.30) | copy-start | bytes 4612
  117.4 5.7 %copy-start.18 = (f32[256]{0:T(256)S(1)}, f32[256]{0:T(256)}, u32[]{:S(2)}) copy-start(f32[256]{0:T(256)} %param.31) | copy-start | bytes 3076
  117.4 43.1 %all-to-all-start.2 = ((bf16[8,768,256]{2,1,0:T(8,128)(2,1)}), bf16[8,768,256]{2,1,0:T(8,128)(2,1)S(1)}, u32[]{:S(2)}, u32[]{:S(2)}) async-start(bf16[8,768,256]{2,1,0:T(8,128)(2,1)} %bitcast.116), calls=%async_computation.2 | async-start | bytes 6291456 | tf_op jit(solution)/shard_map/all_to_all | solution.py:30
  123.1 37.9 %copy-start = (bf16[768,256]{1,0:T(8,128)(2,1)S(1)}, bf16[768,256]{1,0:T(8,128)(2,1)}, u32[]{:S(2)}) copy-start(bf16[768,256]{1,0:T(8,128)(2,1)} %param.24) | copy-start | bytes 1179652
  123.1 46.2 %copy-start.16 = (f32[256]{0:T(256)S(1)}, f32[256]{0:T(256)}, u32[]{:S(2)}) copy-start(f32[256]{0:T(256)} %param.32) | copy-start | bytes 3076
  123.1 75.6 %all-gather.10.cloned.1.call-start = ((), (), s32[]{:S(2)}) async-start(), calls=%async_computation.10 | async-start | bytes 3538944 | tf_op jit(solution)/shard_map/all_gather | solution.py:113
  161.2 15.5 %copy-start.1 = (bf16[768,256]{1,0:T(8,128)(2,1)}, bf16[768,256]{1,0:T(8,128)(2,1)S(1)}, u32[]{:S(2)}) copy-start(bf16[768,256]{1,0:T(8,128)(2,1)S(1)} %get-tuple-element.210) | copy-start | bytes 1179652
  161.2 37.5 %copy-start.24 = (f32[256]{0:T(256)S(1)}, f32[256]{0:T(256)}, u32[]{:S(2)}) copy-start(f32[256]{0:T(256)} %param.38) | copy-start | bytes 3076
  172.3 60.9 %all-to-all-start.4 = ((bf16[16,256,128]{1,2,0:T(8,128)(2,1)}), bf16[16,256,128]{1,2,0:T(8,128)(2,1)}, u32[]{:S(2)}, u32[]{:S(2)}) async-start(bf16[16,256,128]{1,2,0:T(8,128)(2,1)} %broadcast_in_dim.31), calls=%async_computation.4 | async-start | bytes 2097152 | tf_op jit(solution)/shard_map/all_to_all | solution.py:15
  176.7 141.9 %all-gather.14.cloned.1.call-start = ((), (), s32[]{:S(2)}) async-start(), calls=%async_computation.12 | async-start | bytes 3538944 | tf_op jit(solution)/shard_map/all_gather | solution.py:113
  208.9 4.3 %copy-start.26 = (f32[256]{0:T(256)S(1)}, f32[256]{0:T(256)}, u32[]{:S(2)}) copy-start(f32[256]{0:T(256)} %param.39) | copy-start | bytes 3076
  218.5 11.5 %copy-start.27 = (f32[256]{0:T(256)S(1)}, f32[256]{0:T(256)}, u32[]{:S(2)}) copy-start(f32[256]{0:T(256)} %param.40) | copy-start | bytes 3076
  218.5 11.5 %copy-start.28 = (f32[256]{0:T(256)S(1)}, f32[256]{0:T(256)}, u32[]{:S(2)}) copy-start(f32[256]{0:T(256)} %param.41) | copy-start | bytes 3076
  277.1 9.4 %copy-start.17 = (f32[256]{0:T(256)S(1)}, f32[256]{0:T(256)}, u32[]{:S(2)}) copy-start(f32[256]{0:T(256)} %param.45) | copy-start | bytes 3076
  287.4 36.4 %copy-start.23 = (f32[384]{0:T(512)S(1)}, f32[384]{0:T(512)}, u32[]{:S(2)}) copy-start(f32[384]{0:T(512)} %param.30) | copy-start | bytes 4612
  (13 other events, 33.6 us)
Sparse Core Ops, SparseCore 0:
  20.2 32.0 all-gather.5
  54.5 47.8 all-gather.7
  104.5 50.5 all-gather.11
  170.3 28.3 all-gather.9
  287.6 30.9 all-gather.13
where the time goes:
time: 381 us; the launch traced here: 380 us
  waiting for transfers between devices  149 us (39%)
  blocking collectives  109 us (29%)
  matrix products  42.7 us (11%)
  other arithmetic  25.7 us (7%)
  local copies, waits for them, and re-layouts  20.2 us (5%)
  starting transfers between devices  18.2 us (5%)
  between operations  14.5 us (4%)
    all_to_all x2, blocking collectives, sent_and_summed(): lax.all_to_all(in_blocks(shard, dim, length), axis, 0, 0, tiled=True)  82.8 us
    all_gather x3, waiting for transfers between devices, normed_rows(): return lax.all_gather(scaled.astype(jnp.bfloat16), 'tp', axis=1, tiled=True)  61.7 us
    all_gather x2, waiting for transfers between devices, side_by_side(): out = lax.all_gather(both, axis, axis=dim, tiled=True)  50.1 us
    all_to_all x1, waiting for transfers between devices, sent_and_summed(): lax.all_to_all(in_blocks(shard, dim, length), axis, 0, 0, tiled=True)  37.4 us
    all_to_all x3, blocking collectives, from_everyone(): return lax.all_to_all(copies, axis, split_axis=0, concat_axis=0, tiled=True)  26.4 us
    dot_general x2, matrix products, ffn_gathered(): jnp.dot(hidden, gathered_copies(down_low, 'fs', 1), preferred_element_typ...  13.3 us
    dot_general x4, matrix products, per_device(): jnp.dot(features, piece, preferred_element_type=jnp.float32)  12.8 us
    all_to_all x2, starting transfers between devices, from_everyone(): return lax.all_to_all(copies, axis, split_axis=0, concat_axis=0, tiled=True)  12.1 us
  transfers between devices with their start and end apart: 8, of which 5 were waited for; matrix products, arithmetic and copies ran while one was open for 17% of the time, Pallas kernels for 0%

commit v1 on v0

--- a/solution.py
+++ b/solution.py
@@ -8,6 +8,11 @@
 BLK = 128
 EPS = 1e-06
 HEAD_EPS = 0.1
+
+
+def gather_from_all(value, axis, dim):
+    copies = jnp.concatenate([value] * lax.axis_size(axis), axis=dim)
+    return lax.all_to_all(copies, axis, dim, dim, tiled=True)
 
 
 def from_everyone(shard, axis):
@@ -110,7 +115,7 @@
     widened = hidden_in.astype(jnp.float32)
     totals = taken_together(jnp.sum(widened * widened, axis=1), "tp")
     scaled = widened * lax.rsqrt(totals / D + EPS)[:, None] * norm_gain
-    return lax.all_gather(scaled.astype(jnp.bfloat16), "tp", axis=1, tiled=True)
+    return gather_from_all(scaled.astype(jnp.bfloat16), "tp", 1)
 
 
 def summed_share(partial_value):

time: 381 us -> 468 us (1.23)
  local copies, waits for them, and re-layouts: 20.2 us -> 62.8 us
  waiting for transfers between devices: 149 us -> 117 us
  blocking collectives: 109 us -> 140 us
  other arithmetic: 25.7 us -> 49.2 us
  starting transfers between devices: 18.2 us -> 36 us
    all_to_all x0 -> x2, waiting for transfers between devices: none -> 65.3 us  [gather_from_all(): return lax.all_to_all(copies, axis, dim, dim, tiled=True)]
    all_gather x3 -> x0, waiting for transfers between devices: 61.7 us -> none  [normed_rows(): return lax.all_gather(scaled.astype(jnp.bfloat16), 'tp', axis=1, tiled=True)]
    all_gather x2, waiting for transfers between devices: 50.1 us -> 0.01 us  [side_by_side(): out = lax.all_gather(both, axis, axis=dim, tiled=True)]
    all_to_all x0 -> x1, blocking collectives: none -> 42.6 us  [gather_from_all(): return lax.all_to_all(copies, axis, dim, dim, tiled=True)]
    all_to_all x0 -> x6, local copies, waits for them, and re-layouts: none -> 26.3 us  [gather_from_all(): return lax.all_to_all(copies, axis, dim, dim, tiled=True)]
    unnamed x1 -> x22, other arithmetic: 0.01 us -> 22.8 us
    all_to_all x2 -> x3, waiting for transfers between devices: 0.01 us -> 15.4 us  [from_everyone(): return lax.all_to_all(copies, axis, split_axis=0, concat_axis=0, tiled=True)]
    concatenate x0 -> x3, local copies, waits for them, and re-layouts: none -> 12.5 us  [gather_from_all(): copies = jnp.concatenate([value] * lax.axis_size(axis), axis=dim)]
  transfers between devices with their start and end apart: 8 -> 8, of which waited for: 5 -> 5; matrix products, arithmetic and copies ran while one was open for 17% -> 22% of each run, Pallas kernels for 0% -> 0%
where the time goes in v1:
time: 468 us; the launch traced here: 466 us
  blocking collectives  140 us (30%)
  waiting for transfers between devices  117 us (25%)
  local copies, waits for them, and re-layouts  62.8 us (13%)
  other arithmetic  49.2 us (11%)
  matrix products  45 us (10%)
  starting transfers between devices  36 us (8%)
  between operations  14.7 us (3%)
    all_to_all x2, blocking collectives, sent_and_summed(): lax.all_to_all(in_blocks(shard, dim, length), axis, 0, 0, tiled=True)  81.7 us
    all_to_all x2, waiting for transfers between devices, gather_from_all(): return lax.all_to_all(copies, axis, dim, dim, tiled=True)  65.3 us
    all_to_all x1, blocking collectives, gather_from_all(): return lax.all_to_all(copies, axis, dim, dim, tiled=True)  42.6 us
    all_to_all x1, waiting for transfers between devices, sent_and_summed(): lax.all_to_all(in_blocks(shard, dim, length), axis, 0, 0, tiled=True)  36.7 us
    all_to_all x6, local copies, waits for them, and re-layouts, gather_from_all(): return lax.all_to_all(copies, axis, dim, dim, tiled=True)  26.3 us
    unnamed x22, other arithmetic  22.8 us
    all_to_all x3, starting transfers between devices, from_everyone(): return lax.all_to_all(copies, axis, split_axis=0, concat_axis=0, tiled=True)  18.1 us
    all_to_all x2, blocking collectives, from_everyone(): return lax.all_to_all(copies, axis, split_axis=0, concat_axis=0, tiled=True)  16.2 us
  transfers between devices with their start and end apart: 8, of which 5 were waited for; matrix products, arithmetic and copies ran while one was open for 22% of the time, Pallas kernels for 0%

profile of v1, /device:TPU:1, one launch (start us, length us, event | category | flops | bytes accessed | tf_op | source)
XLA Modules:
  0.0 465.8 jit_solution(654511738879370604)
XLA Ops:
  8.4 5.8 %all-to-all-start = ((f32[8,1,768]{2,1,0:T(1,128)}), f32[8,1,768]{2,1,0:T(1,128)S(1)}, u32[]{:S(2)}, u32[]{:S(2)}) async-start(f32[8,1,768]{2,1,0:T(1,128)} %broadcast_in_dim.23), calls=%async_computation | async-start | bytes 49152 | tf_op jit(solution)/shard_map/all_to_all | solution.py:20
  28.9 4.7 %copy.149 = bf16[768,2048]{0,1:T(8,128)(2,1)} copy(bf16[768,2048]{1,0:T(8,128)(2,1)} %constant_dynamic-update-slice_fusion) | data formatting | bytes 6291456 | tf_op jit(solution)/shard_map/concatenate | solution.py:14
  33.6 4.7 %copy.150 = bf16[768,8,256]{2,0,1:T(8,128)(2,1)} copy(bf16[768,8,256]{0,2,1:T(8,128)(2,1)} %bitcast.162) | data formatting | bytes 6291456 | tf_op jit(solution)/shard_map/all_to_all | solution.py:15
  38.3 5.2 %all-to-all-start.1 = ((bf16[768,8,256]{2,0,1:T(8,128)(2,1)}), bf16[768,8,256]{2,0,1:T(8,128)(2,1)}, u32[]{:S(2)}, u32[]{:S(2)}) async-start(bf16[768,8,256]{2,0,1:T(8,128)(2,1)} %copy.150), calls=%async_computation.1 | async-start | bytes 6291456 | tf_op jit(solution)/shard_map/all_to_all | solution.py:15
  43.6 37.4 %all-to-all-done.1 = bf16[768,8,256]{2,0,1:T(8,128)(2,1)} async-done(((bf16[768,8,256]{2,0,1:T(8,128)(2,1)}), bf16[768,8,256]{2,0,1:T(8,128)(2,1)}, u32[]{:S(2)}, u32[]{:S(2)}) %all-to-all-start.1) | async-done | bytes 3145760 | tf_op jit(solution)/shard_map/all_to_all | solution.py:15
  82.3 7.8 %all-to-all-start.2 = ((bf16[16,384,128]{1,2,0:T(8,128)(2,1)}), bf16[16,384,128]{1,2,0:T(8,128)(2,1)S(1)}, u32[]{:S(2)}, u32[]{:S(2)}) async-start(bf16[16,384,128]{1,2,0:T(8,128)(2,1)} %broadcast_in_dim.24), calls=%async_computation.2 | async-start | bytes 3145728 | tf_op jit(solution)/shard_map/all_to_all | solution.py:20
  90.1 4.7 %copy.151 = bf16[768,8,256]{0,2,1:T(8,128)(2,1)} copy(bf16[768,8,256]{2,0,1:T(8,128)(2,1)} %all-to-all-done.1) | data formatting | bytes 6291456 | tf_op jit(solution)/shard_map/all_to_all | solution.py:15
  99.0 13.3 %all-to-all-done.2 = bf16[16,384,128]{1,2,0:T(8,128)(2,1)S(1)} async-done(((bf16[16,384,128]{1,2,0:T(8,128)(2,1)}), bf16[16,384,128]{1,2,0:T(8,128)(2,1)S(1)}, u32[]{:S(2)}, u32[]{:S(2)}) %all-to-all-start.2) | async-done | bytes 1572896 | tf_op jit(solution)/shard_map/all_to_all | solution.py:20
  112.3 8.1 %convolution_convert_fusion.2 = bf16[768,2048]{1,0:T(8,128)(2,1)} fusion(bf16[384,2048]{0,1:T(8,128)(2,1)S(1)} %bitcast.181, bf16[768,2048]{0,1:T(8,128)(2,1)} %bitcast.172, bf16[2048,768]{1,0:T(8,128)(2,1)} %all-gather.3.cloned.1.call-done, f32[768,384]{1,0:T(8,128)S(1)} %convolution_multiply_fusion.4, f32[384]{0:T(512)S(1)} %copy-done.26), kind=kOutput, calls=%fused_computation.38 | convolution fusion | flops 2419556352 | bytes 10618368 | tf_op jit(solution)/shard_map/dot_general | solution.py:131
  124.3 7.6 %all-to-all-start.3 = ((bf16[8,768,256]{2,1,0:T(8,128)(2,1)}), bf16[8,768,256]{2,1,0:T(8,128)(2,1)}, u32[]{:S(2)}, u32[]{:S(2)}) async-start(bf16[8,768,256]{2,1,0:T(8,128)(2,1)} %bitcast.160), calls=%async_computation.3 | async-start | bytes 6291456 | tf_op jit(solution)/shard_map/all_to_all | solution.py:35
  132.8 36.7 %all-to-all-done.3 = bf16[8,768,256]{2,1,0:T(8,128)(2,1)} async-done(((bf16[8,768,256]{2,1,0:T(8,128)(2,1)}), bf16[8,768,256]{2,1,0:T(8,128)(2,1)}, u32[]{:S(2)}, u32[]{:S(2)}) %all-to-all-start.3) | async-done | bytes 3145760 | tf_op jit(solution)/shard_map/all_to_all | solution.py:35
  172.2 8.1 %all_to_all.80 = f32[8,1,768]{2,1,0:T(1,128)S(1)} all-to-all(f32[8,1,768]{2,1,0:T(1,128)S(1)} %broadcast_in_dim.27), channel_id=1, replica_groups=mesh['fs'=16,'tp'=8] {'tp'}, dimensions={0} | all-to-all | bytes 49152 | tf_op jit(solution)/shard_map/all_to_all | solution.py:20
  194.3 5.1 %all-to-all-start.5 = ((bf16[768,8,256]{2,0,1:T(8,128)(2,1)}), bf16[768,8,256]{2,0,1:T(8,128)(2,1)}, u32[]{:S(2)}, u32[]{:S(2)}) async-start(bf16[768,8,256]{2,0,1:T(8,128)(2,1)} %copy.156), calls=%async_computation.5 | async-start | bytes 6291456 | tf_op jit(solution)/shard_map/all_to_all | solution.py:15
  200.6 8.6 %multiply_cosine_fusion = (f32[2,128,256]{1,0,2:T(2,128)}, f32[2,128,256]{1,0,2:T(2,128)}, f32[2,128,256]{1,0,2:T(2,128)}) fusion(f32[2,128]{1,0:T(2,128)S(1)} %multiply_add_fusion, f32[256]{0:T(256)S(1)} %mul.470), kind=kLoop, calls=%fused_computation.107 | loop fusion | flops 327680 | bytes 788480 | tf_op jit(solution)/shard_map/cos | solution.py:75
  209.2 27.8 %all-to-all-done.5 = bf16[768,8,256]{2,0,1:T(8,128)(2,1)} async-done(((bf16[768,8,256]{2,0,1:T(8,128)(2,1)}), bf16[768,8,256]{2,0,1:T(8,128)(2,1)}, u32[]{:S(2)}, u32[]{:S(2)}) %all-to-all-start.5) | async-done | bytes 3145760 | tf_op jit(solution)/shard_map/all_to_all | solution.py:15
  242.6 4.7 %copy.157 = bf16[768,8,256]{0,2,1:T(8,128)(2,1)} copy(bf16[768,8,256]{2,0,1:T(8,128)(2,1)} %all-to-all-done.5) | data formatting | bytes 6291456 | tf_op jit(solution)/shard_map/all_to_all | solution.py:15
  268.1 11.7 %while.15 = (s32[]{:T(128)}, f32[3,1,256,256]{3,2,0,1:T(8,128)S(1)}, f32[2,3,128,1,256]{2,4,1,3,0:T(8,128)}, f32[1]{0:T(128)}, f32[2,3,128,1,256]{2,0,3,4,1:T(2,...) while((s32[]{:T(128)}, ...), condition=%wide.region_6.7_spmd.clone.clone.clone, body=%wide.region_5.6_spmd.clone.clone.clone.sunk | while | flops 152257024 | bytes 7998088 | solution.py:106
  288.3 40.8 %all_to_all.81 = bf16[8,768,256]{2,1,0:T(8,128)(2,1)S(1)} all-to-all(bf16[8,768,256]{2,1,0:T(8,128)(2,1)S(1)} %bitcast.164), channel_id=1, replica_groups=mesh['fs'=16,'tp'=8] {'tp'}, dimensions={0} | all-to-all | bytes 6291456 | tf_op jit(solution)/shard_map/all_to_all | solution.py:35
  330.1 8.1 %all_to_all.82 = f32[8,1,768]{2,1,0:T(1,128)S(1)} all-to-all(f32[8,1,768]{2,1,0:T(1,128)S(1)} %broadcast_in_dim.32), channel_id=1, replica_groups=mesh['fs'=16,'tp'=8] {'tp'}, dimensions={0} | all-to-all | bytes 49152 | tf_op jit(solution)/shard_map/all_to_all | solution.py:20
  350.8 4.7 %copy.173 = bf16[768,8,256]{2,0,1:T(8,128)(2,1)} copy(bf16[768,8,256]{0,2,1:T(8,128)(2,1)} %bitcast.165) | data formatting | bytes 6291456 | tf_op jit(solution)/shard_map/all_to_all | solution.py:15
  355.5 42.6 %all_to_all.83 = bf16[768,8,256]{2,0,1:T(8,128)(2,1)} all-to-all(bf16[768,8,256]{2,0,1:T(8,128)(2,1)} %copy.173), channel_id=1, replica_groups=mesh['fs'=16,'tp'=8] {'tp'}, dimensions={1} | all-to-all | bytes 6291456 | tf_op jit(solution)/shard_map/all_to_all | solution.py:15
  398.1 4.7 %copy.174 = bf16[768,8,256]{0,2,1:T(8,128)(2,1)} copy(bf16[768,8,256]{2,0,1:T(8,128)(2,1)} %all_to_all.83) | data formatting | bytes 6291456 | tf_op jit(solution)/shard_map/all_to_all | solution.py:15
  407.0 7.6 %convolution_convert_fusion = bf16[768,2048]{1,0:T(8,128)(2,1)} fusion(bf16[384,2048]{0,1:T(8,128)(2,1)S(1)} %bitcast.182, bf16[768,2048]{0,1:T(8,128)(2,1)} %bitcast.174, bf16[2048,768]{1,0:T(8,128)(2,1)} %all-gather.3.cloned.1.call-done, f32[768,384]{1,0:T(8,128)S(1)} %convolution_multiply_fusion.2, f32[384]{0:T(512)S(1)} %copy-done.26), kind=kOutput, calls=%fused_computation.36 | convolution fusion | flops 2419556352 | bytes 10618368 | tf_op jit(solution)/shard_map/dot_general | solution.py:131
  416.7 40.9 %all_to_all.84 = bf16[8,768,256]{2,1,0:T(8,128)(2,1)S(1)} all-to-all(bf16[8,768,256]{2,1,0:T(8,128)(2,1)S(1)} %bitcast.166), channel_id=1, replica_groups=mesh['fs'=16,'tp'=8] {'tp'}, dimensions={0} | all-to-all | bytes 6291456 | tf_op jit(solution)/shard_map/all_to_all | solution.py:35
  (177 shorter events, 111.2 us)
Async XLA Ops:
  6.5 16.4 %copy-start = (bf16[768,256]{1,0:T(8,128)(2,1)S(1)}, bf16[768,256]{1,0:T(8,128)(2,1)}, u32[]{:S(2)}) copy-start(bf16[768,256]{1,0:T(8,128)(2,1)} %param.24) | copy-start | bytes 1179652
  6.5 16.4 %copy-start.20 = (f32[256]{0:T(256)S(1)}, f32[256]{0:T(256)}, u32[]{:S(2)}) copy-start(f32[256]{0:T(256)} %param.25) | copy-start | bytes 3076
  8.4 10.5 %all-to-all-start = ((f32[8,1,768]{2,1,0:T(1,128)}), f32[8,1,768]{2,1,0:T(1,128)S(1)}, u32[]{:S(2)}, u32[]{:S(2)}) async-start(f32[8,1,768]{2,1,0:T(1,128)} %broadcast_in_dim.23), calls=%async_computation | async-start | bytes 49152 | tf_op jit(solution)/shard_map/all_to_all | solution.py:20
  14.2 80.6 %all-gather.3.cloned.1.call-start = ((), (), s32[]{:S(2)}) async-start(), calls=%async_computation.11 | async-start | bytes 3342336 | tf_op jit(solution)/shard_map/all_gather | solution.py:42
  38.3 5.2 %copy-start.14 = (f32[384,128]{1,0:T(8,128)S(1)}, f32[384,128]{1,0:T(8,128)}, u32[]{:S(2)}) copy-start(f32[384,128]{1,0:T(8,128)} %param.28) | copy-start | bytes 589828
  38.3 42.7 %all-to-all-start.1 = ((bf16[768,8,256]{2,0,1:T(8,128)(2,1)}), bf16[768,8,256]{2,0,1:T(8,128)(2,1)}, u32[]{:S(2)}, u32[]{:S(2)}) async-start(bf16[768,8,256]{2,0,1:T(8,128)(2,1)} %copy.150), calls=%async_computation.1 | async-start | bytes 6291456 | tf_op jit(solution)/shard_map/all_to_all | solution.py:15
  82.3 30.0 %all-to-all-start.2 = ((bf16[16,384,128]{1,2,0:T(8,128)(2,1)}), bf16[16,384,128]{1,2,0:T(8,128)(2,1)S(1)}, u32[]{:S(2)}, u32[]{:S(2)}) async-start(bf16[16,384,128]{1,2,0:T(8,128)(2,1)} %broadcast_in_dim.24), calls=%async_computation.2 | async-start | bytes 3145728 | tf_op jit(solution)/shard_map/all_to_all | solution.py:20
  90.1 4.7 %copy-start.25 = (f32[384]{0:T(512)S(1)}, f32[384]{0:T(512)}, u32[]{:S(2)}) copy-start(f32[384]{0:T(512)} %param.29) | copy-start | bytes 4612
  94.8 17.5 %copy-start.26 = (f32[384]{0:T(512)S(1)}, f32[384]{0:T(512)}, u32[]{:S(2)}) copy-start(f32[384]{0:T(512)} %param.30) | copy-start | bytes 4612
  112.3 8.2 %copy-start.8 = (bf16[16,384,128]{1,2,0:T(8,128)(2,1)}, bf16[16,384,128]{1,2,0:T(8,128)(2,1)S(1)}, u32[]{:S(2)}) copy-start(bf16[16,384,128]{1,2,0:T(8,128)(2,1)S(1)} %all-to-all-done.2) | copy-start | bytes 4718596
  124.3 7.6 %copy-start.15 = (f32[128,256]{1,0:T(8,128)S(1)}, f32[128,256]{1,0:T(8,128)}, u32[]{:S(2)}) copy-start(f32[128,256]{1,0:T(8,128)} %param.33) | copy-start | bytes 393220
  124.3 7.7 %copy-start.16 = (f32[128,256]{1,0:T(8,128)S(1)}, f32[128,256]{1,0:T(8,128)}, u32[]{:S(2)}) copy-start(f32[128,256]{1,0:T(8,128)} %param.34) | copy-start | bytes 393220
  124.3 7.7 %copy-start.17 = (f32[128,256]{1,0:T(8,128)S(1)}, f32[128,256]{1,0:T(8,128)}, u32[]{:S(2)}) copy-start(f32[128,256]{1,0:T(8,128)} %param.35) | copy-start | bytes 393220
  124.3 7.7 %copy-start.18 = (f32[128,256]{1,0:T(8,128)S(1)}, f32[128,256]{1,0:T(8,128)}, u32[]{:S(2)}) copy-start(f32[128,256]{1,0:T(8,128)} %param.36) | copy-start | bytes 393220
  124.3 8.5 %copy-start.23 = (f32[256]{0:T(256)S(1)}, f32[256]{0:T(256)}, u32[]{:S(2)}) copy-start(f32[256]{0:T(256)} %param.31) | copy-start | bytes 3076
  124.3 45.2 %all-to-all-start.3 = ((bf16[8,768,256]{2,1,0:T(8,128)(2,1)}), bf16[8,768,256]{2,1,0:T(8,128)(2,1)}, u32[]{:S(2)}, u32[]{:S(2)}) async-start(bf16[8,768,256]{2,1,0:T(8,128)(2,1)} %bitcast.160), calls=%async_computation.3 | async-start | bytes 6291456 | tf_op jit(solution)/shard_map/all_to_all | solution.py:35
  131.9 115.4 %all-gather.5.cloned.1.call-start = ((), (), s32[]{:S(2)}) async-start(), calls=%async_computation.12 | async-start | bytes 4456448 | tf_op jit(solution)/shard_map/all_gather | solution.py:42
  132.0 48.3 %copy-start.21 = (f32[256]{0:T(256)S(1)}, f32[256]{0:T(256)}, u32[]{:S(2)}) copy-start(f32[256]{0:T(256)} %param.32) | copy-start | bytes 3076
  194.3 6.2 %copy-start.19 = (f32[256,128]{1,0:T(8,128)S(1)}, f32[256,128]{1,0:T(8,128)}, u32[]{:S(2)}) copy-start(f32[256,128]{1,0:T(8,128)} %param.43) | copy-start | bytes 393220
  194.3 42.7 %all-to-all-start.5 = ((bf16[768,8,256]{2,0,1:T(8,128)(2,1)}), bf16[768,8,256]{2,0,1:T(8,128)(2,1)}, u32[]{:S(2)}, u32[]{:S(2)}) async-start(bf16[768,8,256]{2,0,1:T(8,128)(2,1)} %copy.156), calls=%async_computation.5 | async-start | bytes 6291456 | tf_op jit(solution)/shard_map/all_to_all | solution.py:15
  238.1 47.8 %all-to-all-start.6 = ((bf16[16,256,128]{1,2,0:T(8,128)(2,1)}), bf16[16,256,128]{1,2,0:T(8,128)(2,1)}, u32[]{:S(2)}, u32[]{:S(2)}) async-start(bf16[16,256,128]{1,2,0:T(8,128)(2,1)} %broadcast_in_dim.31), calls=%async_computation.6 | async-start | bytes 2097152 | tf_op jit(solution)/shard_map/all_to_all | solution.py:20
  242.6 4.7 %copy-start.27 = (f32[256]{0:T(256)S(1)}, f32[256]{0:T(256)}, u32[]{:S(2)}) copy-start(f32[256]{0:T(256)} %param.38) | copy-start | bytes 3076
  258.5 4.3 copy-start.29
  329.2 9.0 %copy-start.22 = (f32[256]{0:T(256)S(1)}, f32[256]{0:T(256)}, u32[]{:S(2)}) copy-start(f32[256]{0:T(256)} %param.45) | copy-start | bytes 3076
  (14 other events, 39.8 us)
Sparse Core Ops, SparseCore 0:
  17.1 49.5 all-gather.2
  134.9 48.3 all-gather.4
